TPU v7x, 32 devices: a whole 2x2x4 slice. The times are simulated.
32 devices in a mesh: fs: 4 (over y, x), tp: 8 (over z, core).
Axes of the slice: x: 2, y: 2, z: 4, core: 2. Of those that a mesh axis runs over, the one named last changes fastest.
Arguments:
- normed: bfloat16 [2048, 12288], P('tp', 'fs'), may hold values from -6 to 6
- key_cot: bfloat16 [2048, 12288], P('tp', 'fs'), may hold values from -6 to 6
- first_map: bfloat16 [2048, 12288], P('tp', 'fs'), may hold values from -6 to 6
- second_map: bfloat16 [2048, 12288], P('tp', 'fs'), may hold values from -6 to 6
- lambdas: float32 [8], replicated, may hold values from 0.3 to 0.8
- factor: bfloat16 [2048, 256], replicated, may hold values from -0.125 to 0.125
- key_master: float32 [2048, 2048], P('fs', 'tp'), may hold values from -0.125 to 0.125
- value_master: float32 [2048, 2048], P('fs', 'tp'), may hold values from -0.125 to 0.125
- key_first: float32 [256, 2048], P('fs', 'tp'), may hold values from -6 to 6
- key_second: float32 [256, 2048], P('fs', 'tp'), may hold values from 0.5 to 2
- value_first: float32 [256, 2048], P('fs', 'tp'), may hold values from -6 to 6
- value_second: float32 [256, 2048], P('fs', 'tp'), may hold values from 0.5 to 2
Outputs:
- key_master_new: float32 [2048, 2048], P('fs', 'tp')
- value_master_new: float32 [2048, 2048], P('fs', 'tp')
- key_copy: bfloat16 [2048, 2048], P(None, 'tp')
- value_copy: bfloat16 [2048, 2048], P(None, 'tp')
- key_first_new: float32 [256, 2048], P('fs', 'tp')
- key_second_new: float32 [256, 2048], P('fs', 'tp')
- value_first_new: float32 [256, 2048], P('fs', 'tp')
- value_second_new: float32 [256, 2048], P('fs', 'tp')
All inputs are finite; a program needn't handle non-finite values.
Results may differ from a plain program's by a relative error of at most 0.0012.
Values may be sent and summed in bfloat16 or wider, within the bound.
A program may use at most 64 MiB of HBM per device.

v0:
```python
import math

import jax
import jax.numpy as jnp
from jax import lax
from jax.sharding import PartitionSpec as P

VALUE_DIM = 256


def local(
    normed,
    key_cot,
    first_map,
    second_map,
    lambdas,
    factor,
    key_master,
    value_master,
    key_first,
    key_second,
    value_first,
    value_second,
):
    width = first_map.shape[0]
    key_width = key_cot.shape[0]
    heads = lambdas.shape[0]
    tok_local = normed.shape[1]
    rows_here = lax.axis_index("tp") * width + lax.iota(jnp.int32, width)
    owners = rows_here // VALUE_DIM
    picked = (owners[:, None] == lax.iota(jnp.int32, heads)[None, :]).astype(jnp.float32)
    row_lambda = jnp.sum(picked * lambdas[None, :], axis=1)
    value_cot = (
        first_map.astype(jnp.float32) - row_lambda[:, None] * second_map.astype(jnp.float32)
    ).astype(jnp.bfloat16)
    cotangents = jnp.concatenate([key_cot, value_cot], axis=0)
    norm_scale = 1.0 / math.sqrt(tok_local * lax.axis_size("fs"))
    fs_rows = key_master.shape[0]
    factor_rows = lax.dynamic_slice_in_dim(
        factor, lax.axis_index("fs") * fs_rows, fs_rows, 0
    ).astype(jnp.float32)
    feature_rows = normed.shape[0]
    factor_cols = lax.dynamic_slice_in_dim(
        factor, lax.axis_index("tp") * feature_rows, feature_rows, 0
    )
    share = lax.psum_scatter(
        lax.dot_general(
            normed, factor_cols, (((0,), (0,)), ((), ())), preferred_element_type=jnp.float32
        ),
        "tp",
        scatter_dimension=0,
        tiled=True,
    )
    projected = lax.all_gather(share, "tp", axis=0, tiled=True)
    partial_value = (
        lax.dot_general(
            projected,
            cotangents.astype(jnp.float32),
            (((0,), (1,)), ((), ())),
            precision=lax.Precision.HIGHEST,
        )
        * norm_scale
    )
    small = lax.psum_scatter(partial_value, "fs", scatter_dimension=0, tiled=True)
    first = jnp.concatenate([key_first, value_first], axis=1)
    second = jnp.concatenate([key_second, value_second], axis=1)
    first_new = 0.8 * first + 0.2 * small
    second_new = 0.9 * second + 0.1 * small * small
    direction = first_new / (jnp.sqrt(second_new) + 1e-06)
    directions = lax.all_gather(direction, "fs", axis=0, tiled=True)
    raw = jnp.dot(factor_rows, directions, precision=lax.Precision.HIGHEST)
    key_raw = raw[:, :key_width]
    value_raw = raw[:, key_width:]
    squares = lax.psum((jnp.sum(key_raw * key_raw), jnp.sum(value_raw * value_raw)), ("fs", "tp"))
    key_cells = fs_rows * lax.axis_size("fs") * key_width * lax.axis_size("tp")
    value_cells = fs_rows * lax.axis_size("fs") * width * lax.axis_size("tp")
    key_update = key_raw / jnp.sqrt(squares[0] / key_cells + 0.01)
    value_update = value_raw / jnp.sqrt(squares[1] / value_cells + 0.01)
    key_new = 0.998 * key_master - 0.02 * key_update
    value_new = 0.998 * value_master - 0.02 * value_update
    halves = jnp.concatenate([key_new, value_new], axis=1).astype(jnp.bfloat16)
    copies = lax.all_gather(halves, "fs", axis=0, tiled=True)
    return (
        key_new,
        value_new,
        copies[:, :key_width],
        copies[:, key_width:],
        first_new[:, :key_width],
        second_new[:, :key_width],
        first_new[:, key_width:],
        second_new[:, key_width:],
    )


def solution(mesh):
    in_specs = (
        P("tp", "fs"),
        P("tp", "fs"),
        P("tp", "fs"),
        P("tp", "fs"),
        P(),
        P(),
        P("fs", "tp"),
        P("fs", "tp"),
        P("fs", "tp"),
        P("fs", "tp"),
        P("fs", "tp"),
        P("fs", "tp"),
    )
    out_specs = (
        P("fs", "tp"),
        P("fs", "tp"),
        P(None, "tp"),
        P(None, "tp"),
        P("fs", "tp"),
        P("fs", "tp"),
        P("fs", "tp"),
        P("fs", "tp"),
    )
    return jax.shard_map(local, mesh=mesh, in_specs=in_specs, out_specs=out_specs, check_vma=False)
```

profile of v0, /device:TPU:0, one launch (start us, length us, event | category | flops | bytes accessed | tf_op | source)
XLA Modules:
  0.0 230.3 jit_solution(11206686593514664223)
XLA Ops:
  7.2 0.0 reduce-scatter.3.cloned.1.call-start
  7.2 1.3 copy-done
  8.6 3.3 %convolution_bitcast_fusion = f32[3072,256]{0,1:T(8,128)} fusion(bf16[256,3072]{1,0:T(8,128)(2,1)S(1)} %copy-done, bf16[2048,256]{1,0:T(8,128)(2,1)} %param.17, s32[]{:T(128)S(6)} %select_n.16), kind=kOutput, calls=%fused_computation | convolution fusion | flops 402653184 | bytes 4849668 | tf_op jit(solution)/shard_map/dot_general | solution.py:47
  11.9 0.0 reduce-scatter.3.cloned.1.call-update
  11.9 0.0 all-gather.3.cloned.1.call-start
  11.9 43.2 %reduce-scatter.3.cloned.1.call-done = f32[384,256]{0,1:T(8,128)} async-done(((f32[3072,256]{0,1:T(8,128)}), f32[384,256]{0,1:T(8,128)}) %reduce-scatter.3.cloned.1.call-update) | async-done | bytes 393232 | tf_op jit(solution)/shard_map/reduce_scatter | solution.py:46
  55.1 0.0 all-gather.3.cloned.1.call-update
  55.1 0.0 reduce-scatter.5.cloned.1.call-start
  55.2 0.1 select_reduce_fusion
  55.3 3.3 %subtract_convert_fusion = bf16[256,3072]{1,0:T(8,128)(2,1)} fusion(bf16[256,3072]{1,0:T(8,128)(2,1)S(1)} %copy-done.1, bf16[256,3072]{1,0:T(8,128)(2,1)} %param.14, f32[256]{0:T(256)S(1)} %select_reduce_fusion), kind=kLoop, calls=%fused_computation.5 | loop fusion | flops 3932160 | bytes 4719616 | tf_op jit(solution)/shard_map/convert_element_type | solution.py:35
  58.6 35.7 %all-gather.3.cloned.1.call-done = f32[3072,256]{0,1:T(8,128)} async-done(((f32[384,256]{0,1:T(8,128)}), f32[3072,256]{0,1:T(8,128)}) %all-gather.3.cloned.1.call-update) | async-done | bytes 3145744 | tf_op jit(solution)/shard_map/all_gather | solution.py:54
  94.3 6.3 %fusion.4 = f32[256,512]{1,0:T(8,128)} fusion(f32[3072,256]{0,1:T(8,128)} %all-gather.3.cloned.1.call-done, bf16[256,3072]{1,0:T(8,128)(2,1)} %subtract_convert_fusion, bf16[256,3072]{1,0:T(8,128)(2,1)} %param.13), kind=kOutput, calls=%fused_computation.6 | convolution fusion | flops 4838260736 | bytes 6815744 | tf_op jit(solution)/shard_map/dot_general | solution.py:56
  100.6 0.0 reduce-scatter.5.cloned.1.call-update
  100.6 0.0 all-gather.5.cloned.1.call-start
  100.6 0.2 copy.27
  100.9 1.0 copy.26
  101.9 22.9 %reduce-scatter.5.cloned.1.call-done = f32[64,512]{1,0:T(8,128)} async-done(((f32[256,512]{1,0:T(8,128)}), f32[64,512]{1,0:T(8,128)}) %reduce-scatter.5.cloned.1.call-update) | async-done | bytes 131088 | tf_op jit(solution)/shard_map/reduce_scatter | solution.py:64
  124.7 1.0 add_divide_fusion
  125.8 10.3 %all_gather.10 = f32[256,512]{1,0:T(8,128)S(1)} all-gather(f32[64,512]{1,0:T(8,128)S(1)} %get-tuple-element.32), channel_id=1, replica_groups=mesh['fs'=4,'tp'=8] {'fs'}, dimensions={0}, use_global_device_ids=true | all-gather | bytes 655360 | tf_op jit(solution)/shard_map/all_gather | solution.py:70
  136.0 1.6 fusion.7
  137.6 0.7 multiply_reduce_fusion
  138.4 39.5 %all-reduce = (f32[]{:T(128)}, f32[]{:T(128)}) all-reduce(f32[]{:T(128)} %get-tuple-element.25, f32[]{:T(128)} %get-tuple-element.24), channel_id=1, replica_groups=mesh['fs'=4,'tp'=8] {'fs','tp'}, use_global_device_ids=true, to_apply=%region_4.5 | all-reduce | flops 2 | bytes 16 | tf_op jit(solution)/shard_map/psum | solution.py:74
  179.3 2.3 fusion.16
  181.5 0.8 pad_maximum_fusion
  182.4 0.0 all-gather.5.cloned.1.call-update
  182.4 2.0 copy.28
  184.4 2.0 copy.29
  186.5 0.7 fusion.20
  187.2 30.4 %all-gather.5.cloned.1.call-done = bf16[2048,512]{0,1:T(8,128)(2,1)} async-done(((bf16[512,512]{0,1:T(8,128)(2,1)}), bf16[2048,512]{0,1:T(8,128)(2,1)}) %all-gather.5.cloned.1.call-update) | async-done | bytes 2097168 | tf_op jit(solution)/shard_map/all_gather | solution.py:82
  217.5 2.7 %fusion.19 = (bf16[2048,256]{0,1:T(8,128)(2,1)S(1)}, bf16[2048,256]{0,1:T(8,128)(2,1)}) fusion(bf16[2048,512]{0,1:T(8,128)(2,1)} %all-gather.5.cloned.1.call-done), kind=kLoop, calls=%fused_computation.32 | loop fusion | bytes 4194304 | tf_op jit(solution)/shard_map/slice | solution.py:87
  220.2 2.3 copy.30
  222.5 1.3 copy.31
  (14 shorter events, 0.0 us)
Async XLA Ops:
  7.2 1.4 copy-start
  7.2 47.9 %reduce-scatter.3.cloned.1.call-start = ((), (), s32[]{:S(2)}) async-start(), calls=%async_computation.2 | async-start | bytes 3538944 | tf_op jit(solution)/shard_map/reduce_scatter | solution.py:46
  8.6 46.6 %copy-start.6 = (f32[8]{0:T(128)S(1)}, f32[8]{0:T(128)}, u32[]{:S(2)}) copy-start(f32[8]{0:T(128)} %param.16) | copy-start | bytes 100
  8.6 46.7 %copy-start.1 = (bf16[256,3072]{1,0:T(8,128)(2,1)S(1)}, bf16[256,3072]{1,0:T(8,128)(2,1)}, u32[]{:S(2)}) copy-start(bf16[256,3072]{1,0:T(8,128)(2,1)} %param.15) | copy-start | bytes 4718596
  11.9 82.4 %all-gather.3.cloned.1.call-start = ((), (), s32[]{:S(2)}) async-start(), calls=%async_computation.3 | async-start | bytes 3538944 | tf_op jit(solution)/shard_map/all_gather | solution.py:54
  55.1 69.6 %reduce-scatter.5.cloned.1.call-start = ((), (), s32[]{:S(2)}) async-start(), calls=%async_computation.4 | async-start | bytes 655360 | tf_op jit(solution)/shard_map/reduce_scatter | solution.py:64
  58.6 42.0 %copy-start.2 = (f32[512,256]{1,0:T(8,128)S(1)}, f32[512,256]{1,0:T(8,128)}, u32[]{:S(2)}) copy-start(f32[512,256]{1,0:T(8,128)} %param.19) | copy-start | bytes 1572868
  58.6 42.2 %copy-start.3 = (f32[512,256]{1,0:T(8,128)S(1)}, f32[512,256]{1,0:T(8,128)}, u32[]{:S(2)}) copy-start(f32[512,256]{1,0:T(8,128)} %param.18) | copy-start | bytes 1572868
  58.6 66.1 %copy-start.4 = (f32[64,256]{1,0:T(8,128)S(1)}, f32[64,256]{1,0:T(8,128)}, u32[]{:S(2)}) copy-start(f32[64,256]{1,0:T(8,128)} %param.23) | copy-start | bytes 196612
  58.6 66.1 %copy-start.5 = (f32[64,256]{1,0:T(8,128)S(1)}, f32[64,256]{1,0:T(8,128)}, u32[]{:S(2)}) copy-start(f32[64,256]{1,0:T(8,128)} %param.21) | copy-start | bytes 196612
  100.6 117.0 %all-gather.5.cloned.1.call-start = ((), (), s32[]{:S(2)}) async-start(), calls=%async_computation.5 | async-start | bytes 2621440 | tf_op jit(solution)/shard_map/all_gather | solution.py:82
Sparse Core Ops, SparseCore 0:
  12.0 43.0 reduce-scatter.2
  56.7 37.5 all-gather.2
  100.7 23.9 reduce-scatter.4
  182.5 34.9 all-gather.4
where the time goes:
time: 231 us; the launch traced here: 230 us
  waiting for transfers between devices  132 us (57%)
  blocking collectives  49.8 us (22%)
  between operations  15.2 us (7%)
  local copies, waits for them, and re-layouts  13.6 us (6%)
  matrix products  11.1 us (5%)
  other arithmetic  8.26 us (4%)
    reduce_scatter x1, waiting for transfers between devices, local(): lax.psum_scatter(lax.dot_general(normed, factor_cols, (((0,), (0,)), ((),...  43.2 us
    psum x1, blocking collectives, local(): lax.psum((jnp.sum(key_raw * key_raw), jnp.sum(value_raw * value_raw)), ('...  39.5 us
    all_gather x1, waiting for transfers between devices, local(): projected = lax.all_gather(share, 'tp', axis=0, tiled=True)  35.7 us
    all_gather x1, waiting for transfers between devices, local(): copies = lax.all_gather(halves, 'fs', axis=0, tiled=True)  30.4 us
    reduce_scatter x1, waiting for transfers between devices, local(): lax.psum_scatter(partial_value, 'fs', scatter_dimension=0, tiled=True)  22.9 us
    all_gather x1, blocking collectives, local(): directions = lax.all_gather(direction, 'fs', axis=0, tiled=True)  10.3 us
    unnamed x20, local copies, waits for them, and re-layouts  10.2 us
    dot_general x1, matrix products, local(): lax.dot_general(projected, cotangents.astype(jnp.float32), (((0,), (1,)),...  6.26 us
  transfers between devices with their start and end apart: 4, of which 4 were waited for; matrix products, arithmetic and copies ran while one was open for 4% of the time, Pallas kernels for 0%

commit v1 on v0

v1 whole, which is shorter than its diff:
```python
import functools
import math

import jax
import jax.numpy as jnp
from jax import lax
from jax.experimental import pallas as pl
from jax.experimental.pallas import tpu as pltpu
from jax.sharding import PartitionSpec as P

VALUE_DIM = 256
CORES = 2
LANES = 128
LAG = 3
MESH = pl.DeviceIdType.MESH
F32 = jnp.float32
BF16 = jnp.bfloat16


def flipped(index, bit):
    step = 1 << bit
    return index + step * (1 - 2 * ((index // step) % 2))


def split(value):
    high = value.astype(BF16)
    return high, (value - high.astype(F32)).astype(BF16)


def kernel(
    n_fs,
    n_tp,
    scale,
    normed,
    key_cot,
    first_map,
    second_map,
    lambdas,
    factor,
    key_master,
    value_master,
    key_first,
    key_second,
    value_first,
    value_second,
    key_new,
    value_new,
    key_copy,
    value_copy,
    key_first_new,
    key_second_new,
    value_first_new,
    value_second_new,
    x_v,
    kc_v,
    vc_v,
    sm_v,
    fac_v,
    ft_v,
    mom_v,
    own,
    away,
    sib,
    left,
    right,
    right_out,
    proj,
    key_acc,
    value_acc,
    masters,
    raw,
    copies,
    part,
    part_in,
    moved,
    dirs,
    norms,
    in_sem,
    sib_s,
    sib_r,
    left_s,
    left_r,
    right_s,
    right_r,
    proj_s,
    proj_r,
    mast_s,
    mast_r,
    part_s,
    part_r,
    dir_s,
    dir_r,
    norm_s,
    norm_r,
    out_sem,
):
    fs = lax.axis_index("fs")
    tp = lax.axis_index("tp")
    z = tp // CORES
    core = tp % CORES
    n_z = n_tp // CORES
    features = normed.shape[0]
    width = first_map.shape[0]
    rank = factor.shape[1]
    pieces = own.shape[0]
    subs, sub_rows = left.shape[0] // pieces, left.shape[1]
    steps = pieces * subs
    fs_rows = key_master.shape[0]
    rank_rows = rank // n_fs
    bits = n_fs.bit_length() - 1
    other = z * CORES + (1 - core)

    loads = [
        pltpu.make_async_copy(normed, x_v, in_sem.at[0]),
        pltpu.make_async_copy(factor, fac_v, in_sem.at[1]),
        pltpu.make_async_copy(first_map, vc_v, in_sem.at[2]),
        pltpu.make_async_copy(second_map, sm_v, in_sem.at[3]),
        pltpu.make_async_copy(key_cot, kc_v, in_sem.at[4]),
        pltpu.make_async_copy(key_master, masters.at[0, fs], in_sem.at[5]),
        pltpu.make_async_copy(value_master, masters.at[1, fs], in_sem.at[6]),
        pltpu.make_async_copy(key_first, mom_v.at[0], in_sem.at[7]),
        pltpu.make_async_copy(value_first, mom_v.at[1], in_sem.at[8]),
        pltpu.make_async_copy(key_second, mom_v.at[2], in_sem.at[9]),
        pltpu.make_async_copy(value_second, mom_v.at[3], in_sem.at[10]),
    ]
    for load in loads:
        load.start()

    barrier = pltpu.get_barrier_semaphore()
    for d in range(1, n_fs):
        pl.semaphore_signal(
            barrier, inc=1, device_id=(lax.rem(fs + d, n_fs), tp), device_id_type=MESH
        )
    for d in range(1, n_tp):
        pl.semaphore_signal(
            barrier, inc=1, device_id=(fs, lax.rem(tp + d, n_tp)), device_id_type=MESH
        )
    pl.semaphore_wait(barrier, n_fs + n_tp - 2)

    def master_copy(kv, step, j):
        order = list(range(bits)) if kv == 0 else list(range(bits))[::-1]
        block = fs
        for t in range(step):
            if (j >> t) & 1:
                block = flipped(block, order[t])
        if j == 0:
            src = (key_master, value_master)[kv]
        else:
            src = masters.at[kv, block]
        slot = (1 << step) - 1 + j
        return pltpu.make_async_remote_copy(
            src_ref=src,
            dst_ref=masters.at[kv, block],
            send_sem=mast_s.at[kv, slot],
            recv_sem=mast_r.at[kv, slot],
            device_id=(flipped(fs, order[step]), tp),
            device_id_type=MESH,
        )

    for step in range(bits):
        for kv in range(2):
            master_copy(kv, step, 0).start()

    def wait_masters(step):
        for kv in range(2):
            for j in range(1 << step):
                master_copy(kv, step, j).wait_recv()

    def sib_copy(k):
        return pltpu.make_async_remote_copy(
            src_ref=away.at[k],
            dst_ref=sib.at[k],
            send_sem=sib_s.at[k],
            recv_sem=sib_r.at[k],
            device_id=(fs, other),
            device_id_type=MESH,
        )

    def left_copy(s):
        return pltpu.make_async_remote_copy(
            src_ref=left.at[s],
            dst_ref=left.at[s],
            send_sem=left_s.at[s],
            recv_sem=left_r.at[s],
            device_id=(fs, lax.rem(tp + CORES, n_tp)),
            device_id_type=MESH,
        )

    def right_copy(s):
        return pltpu.make_async_remote_copy(
            src_ref=right_out.at[s],
            dst_ref=right.at[s],
            send_sem=right_s.at[s],
            recv_sem=right_r.at[s],
            device_id=(fs, lax.rem(tp + n_tp - CORES, n_tp)),
            device_id_type=MESH,
        )

    def proj_copy(k):
        return pltpu.make_async_remote_copy(
            src_ref=proj.at[core * pieces + k],
            dst_ref=proj.at[core * pieces + k],
            send_sem=proj_s.at[k],
            recv_sem=proj_r.at[k],
            device_id=(fs, other),
            device_id_type=MESH,
        )

    loads[0].wait()
    loads[1].wait()
    ft_v[...] = fac_v[pl.ds(pl.multiple_of(tp * features, features), features), :].astype(F32).T.astype(BF16)

    def project(side, k):
        cols = pl.ds(pl.multiple_of((side * pieces + k) * LANES, LANES), LANES)
        return jnp.dot(ft_v[...], x_v[:, cols], preferred_element_type=F32)

    @pl.loop(0, pieces)
    def _(k):
        away[k] = project(1 - core, k)
        sib_copy(k).start()
        own[k] = project(core, k)

    loads[2].wait()
    loads[3].wait()
    span = math.gcd(width, VALUE_DIM)
    for b in range(width // span):
        row_lambda = lambdas[(tp * width + b * span) // VALUE_DIM]

        @pl.loop(0, vc_v.shape[1] // LANES)
        def _(c):
            at = (pl.ds(b * span, span), pl.ds(pl.multiple_of(c * LANES, LANES), LANES))
            vc_v[at] = (vc_v[at].astype(F32) - row_lambda * sm_v[at].astype(F32)).astype(BF16)

    loads[4].wait()
    key_acc[...] = jnp.zeros_like(key_acc)
    value_acc[...] = jnp.zeros_like(value_acc)

    def accumulate(piece):
        cols = pl.ds(pl.multiple_of(piece * LANES, LANES), LANES)
        dims = (((1,), (1,)), ((), ()))
        key_acc[...] += lax.dot_general(
            proj[piece], kc_v[:, cols], dims, preferred_element_type=F32
        )
        value_acc[...] += lax.dot_general(
            proj[piece], vc_v[:, cols], dims, preferred_element_type=F32
        )

    def sibling_piece(k):
        return (1 - core) * pieces + k

    def accumulate_sibling(k):
        pltpu.make_async_remote_copy(
            src_ref=proj.at[sibling_piece(k)],
            dst_ref=proj.at[sibling_piece(k)],
            send_sem=proj_s.at[k],
            recv_sem=proj_r.at[k],
            device_id=(fs, other),
            device_id_type=MESH,
        ).wait_recv()
        accumulate(sibling_piece(k))

    def rows_of(s):
        return pl.ds(pl.multiple_of((s % subs) * sub_rows, sub_rows), sub_rows)

    @pl.loop(0, steps + LAG * (n_z - 1))
    def _(i):
        @pl.when(jnp.logical_and(i < steps, i % subs == 0))
        def _():
            k = i // subs
            sib_copy(k).wait_recv()
            own[k] = own[k] + sib[k]

        s_left = i - LAG * z

        @pl.when(jnp.logical_and(s_left >= 0, s_left < steps))
        def _():
            total = own[s_left // subs, rows_of(s_left), :]

            @pl.when(z > 0)
            def _():
                left_copy(s_left).wait_recv()
                left[s_left] = left[s_left] + total

            @pl.when(z == 0)
            def _():
                left[s_left] = total

            @pl.when(z < n_z - 1)
            def _():
                left_copy(s_left).start()

        s_right = i - LAG * (n_z - 1 - z)

        @pl.when(jnp.logical_and(s_right >= 0, s_right < steps))
        def _():
            total = own[s_right // subs, rows_of(s_right), :]

            @pl.when(z < n_z - 1)
            def _():
                right_copy(s_right).wait_recv()

                @pl.when(z > 0)
                def _():
                    right_out[s_right] = right[s_right] + total

            @pl.when(z == n_z - 1)
            def _():
                right[s_right] = jnp.zeros_like(total)

                @pl.when(z > 0)
                def _():
                    right_out[s_right] = total

            @pl.when(z > 0)
            def _():
                right_copy(s_right).start()

        s_done = i - LAG * jnp.maximum(z, n_z - 1 - z)

        @pl.when(jnp.logical_and(s_done >= 0, s_done < steps))
        def _():
            k = s_done // subs
            mine = core * pieces + k
            high, low = split(left[s_done] + right[s_done])
            proj[mine, rows_of(s_done), :] = high
            proj[mine, pl.ds(pl.multiple_of(rank + (s_done % subs) * sub_rows, sub_rows), sub_rows), :] = low

            @pl.when(s_done % subs == subs - 1)
            def _():
                proj_copy(k).start()
                accumulate(mine)

                @pl.when(k > 0)
                def _():
                    accumulate_sibling(k - 1)

        for t in range(1, bits):

            @pl.when(i == (steps * t) // bits)
            def _():
                wait_masters(t - 1)
                for j in range(1, 1 << t):
                    for kv in range(2):
                        master_copy(kv, t, j).start()

    accumulate_sibling(pieces - 1)

    for j in range(n_fs):
        rows = pl.ds(j * rank_rows, rank_rows)
        lows = pl.ds(rank + j * rank_rows, rank_rows)
        part[j, 0] = (key_acc[rows, :] + key_acc[lows, :]) * scale
        part[j, 1] = (value_acc[rows, :] + value_acc[lows, :]) * scale

    def part_copy(d):
        to = lax.rem(fs + d, n_fs)
        return pltpu.make_async_remote_copy(
            src_ref=part.at[to],
            dst_ref=part_in.at[d - 1],
            send_sem=part_s.at[d - 1],
            recv_sem=part_r.at[d - 1],
            device_id=(to, tp),
            device_id_type=MESH,
        )

    def dir_copy(d):
        return pltpu.make_async_remote_copy(
            src_ref=dirs.at[fs],
            dst_ref=dirs.at[fs],
            send_sem=dir_s.at[d - 1],
            recv_sem=dir_r.at[d - 1],
            device_id=(lax.rem(fs + d, n_fs), tp),
            device_id_type=MESH,
        )

    def norm_copy(d):
        return pltpu.make_async_remote_copy(
            src_ref=norms.at[0],
            dst_ref=norms.at[d],
            send_sem=norm_s.at[d - 1],
            recv_sem=norm_r.at[d - 1],
            device_id=(fs, lax.rem(tp + d, n_tp)),
            device_id_type=MESH,
        )

    for d in range(1, n_fs):
        part_copy(d).start()
    for load in loads[7:]:
        load.wait()
    small = part[fs]
    for d in range(1, n_fs):
        part_copy(d).wait_recv()
        small = small + part_in[d - 1]
    first_new = 0.8 * mom_v[0:2] + 0.2 * small
    second_new = 0.9 * mom_v[2:4] + 0.1 * small * small
    dirs[fs] = first_new / (jnp.sqrt(second_new) + 1e-06)
    for d in range(1, n_fs):
        dir_copy(d).start()
    moved[0:2] = first_new
    moved[2:4] = second_new
    moments = [
        pltpu.make_async_copy(moved.at[n], ref, out_sem.at[n])
        for n, ref in enumerate((key_first_new, value_first_new, key_second_new, value_second_new))
    ]
    for copy in moments:
        copy.start()
    for load in loads[5:7]:
        load.wait()
    for d in range(1, n_fs):
        pltpu.make_async_remote_copy(
            src_ref=dirs.at[lax.rem(fs + n_fs - d, n_fs)],
            dst_ref=dirs.at[lax.rem(fs + n_fs - d, n_fs)],
            send_sem=dir_s.at[d - 1],
            recv_sem=dir_r.at[d - 1],
            device_id=(lax.rem(fs + d, n_fs), tp),
            device_id_type=MESH,
        ).wait_recv()

    block = fs_rows
    sums = []
    for kv in range(2):
        high, low = split(jnp.concatenate([dirs[j, kv] for j in range(n_fs)], axis=0))

        def body(n, total):
            rows = fac_v[pl.ds(pl.multiple_of(n * block, block), block), :]
            out = jnp.dot(rows, high, preferred_element_type=F32) + jnp.dot(
                rows, low, preferred_element_type=F32
            )
            raw[kv, n] = out
            return total + jnp.sum((out * out).reshape(block // 8, 8, width), axis=0)

        total = lax.fori_loop(0, n_fs, body, jnp.zeros((8, width), F32))
        sums.append(jnp.sum(total))
    norms[0, 0] = jnp.full(norms.shape[2:], sums[0], F32)
    norms[0, 1] = jnp.full(norms.shape[2:], sums[1], F32)
    for d in range(1, n_tp):
        norm_copy(d).start()
    wait_masters(bits - 1)
    squares = norms[0]
    for d in range(1, n_tp):
        norm_copy(d).wait_recv()
        squares = squares + norms[d]
    cells = factor.shape[0] * width * n_tp
    factors = 0.02 / jnp.sqrt(squares / cells + 0.01)

    def copy_out(kv, n):
        rows = pl.ds(pl.multiple_of(n * block, block), block)
        return pltpu.make_async_copy(
            copies.at[kv, n], (key_copy, value_copy)[kv].at[rows, :], out_sem.at[4 + kv * (n_fs + 1) + n]
        )

    def new_out(kv):
        return pltpu.make_async_copy(
            raw.at[kv, fs], (key_new, value_new)[kv], out_sem.at[4 + kv * (n_fs + 1) + n_fs]
        )

    for kv in range(2):
        grain = factors[kv, 0:1, 0:1]

        @pl.loop(0, n_fs)
        def _(n):
            new = 0.998 * masters[kv, n] - grain * raw[kv, n]
            raw[kv, n] = new
            copies[kv, n] = new.astype(BF16)
            copy_out(kv, n).start()

        new_out(kv).start()

    @pl.loop(0, pieces)
    def _(k):
        sib_copy(k).wait_send()
        proj_copy(k).wait_send()

    @pl.loop(0, steps)
    def _(s):
        @pl.when(z < n_z - 1)
        def _():
            left_copy(s).wait_send()

        @pl.when(z > 0)
        def _():
            right_copy(s).wait_send()

    for kv in range(2):
        for step in range(bits):
            for j in range(1 << step):
                master_copy(kv, step, j).wait_send()
    for d in range(1, n_fs):
        part_copy(d).wait_send()
        dir_copy(d).wait_send()
    for d in range(1, n_tp):
        norm_copy(d).wait_send()
    for copy in moments:
        copy.wait()
    for kv in range(2):
        for n in range(n_fs):
            copy_out(kv, n).wait()
        new_out(kv).wait()


def local(n_fs, n_tp, *args):
    normed, key_cot, first_map, second_map, lambdas, factor, key_master = args[:7]
    features, tokens = normed.shape
    width = first_map.shape[0]
    rows, rank = factor.shape
    fs_rows = key_master.shape[0]
    rank_rows = rank // n_fs
    pieces = tokens // (CORES * LANES)
    subs = 2
    steps = pieces * subs
    sub_rows = rank // subs
    scale = 1.0 / math.sqrt(tokens * n_fs)
    any_spec = pl.BlockSpec(memory_space=pl.ANY)
    specs = [any_spec] * 12
    specs[4] = pl.BlockSpec(memory_space=pltpu.SMEM)
    dma = pltpu.SemaphoreType.DMA
    sds = jax.ShapeDtypeStruct
    small = sds((rank_rows, width), F32)
    return pl.pallas_call(
        functools.partial(kernel, n_fs, n_tp, scale),
        out_shape=[
            sds((fs_rows, width), F32),
            sds((fs_rows, width), F32),
            sds((rows, width), BF16),
            sds((rows, width), BF16),
            small,
            small,
            small,
            small,
        ],
        in_specs=specs,
        out_specs=[any_spec] * 8,
        scratch_shapes=[
            pltpu.VMEM((features, tokens), BF16),
            pltpu.VMEM((width, tokens), BF16),
            pltpu.VMEM((width, tokens), BF16),
            pltpu.VMEM((width, tokens), BF16),
            pltpu.VMEM((rows, rank), BF16),
            pltpu.VMEM((rank, features), BF16),
            pltpu.VMEM((4, rank_rows, width), F32),
            pltpu.VMEM((pieces, rank, LANES), F32),
            pltpu.VMEM((pieces, rank, LANES), F32),
            pltpu.VMEM((pieces, rank, LANES), F32),
            pltpu.VMEM((steps, sub_rows, LANES), F32),
            pltpu.VMEM((steps, sub_rows, LANES), F32),
            pltpu.VMEM((steps, sub_rows, LANES), F32),
            pltpu.VMEM((CORES * pieces, 2 * rank, LANES), BF16),
            pltpu.VMEM((2 * rank, width), F32),
            pltpu.VMEM((2 * rank, width), F32),
            pltpu.VMEM((2, n_fs, fs_rows, width), F32),
            pltpu.VMEM((2, n_fs, fs_rows, width), F32),
            pltpu.VMEM((2, n_fs, fs_rows, width), BF16),
            pltpu.VMEM((n_fs, 2, rank_rows, width), F32),
            pltpu.VMEM((n_fs - 1, 2, rank_rows, width), F32),
            pltpu.VMEM((4, rank_rows, width), F32),
            pltpu.VMEM((n_fs, 2, rank_rows, width), F32),
            pltpu.VMEM((n_tp, 2, 8, LANES), F32),
            dma((11,)),
            dma((pieces,)),
            dma((pieces,)),
            dma((steps,)),
            dma((steps,)),
            dma((steps,)),
            dma((steps,)),
            dma((pieces,)),
            dma((pieces,)),
            dma((2, n_fs - 1)),
            dma((2, n_fs - 1)),
            dma((n_fs - 1,)),
            dma((n_fs - 1,)),
            dma((n_fs - 1,)),
            dma((n_fs - 1,)),
            dma((n_tp - 1,)),
            dma((n_tp - 1,)),
            dma((4 + 2 * (n_fs + 1),)),
        ],
        compiler_params=pltpu.CompilerParams(
            collective_id=0, has_side_effects=True, vmem_limit_bytes=60 * 1024 * 1024
        ),
    )(*args)


def solution(mesh):
    in_specs = (
        P("tp", "fs"),
        P("tp", "fs"),
        P("tp", "fs"),
        P("tp", "fs"),
        P(),
        P(),
        P("fs", "tp"),
        P("fs", "tp"),
        P("fs", "tp"),
        P("fs", "tp"),
        P("fs", "tp"),
        P("fs", "tp"),
    )
    out_specs = (
        P("fs", "tp"),
        P("fs", "tp"),
        P(None, "tp"),
        P(None, "tp"),
        P("fs", "tp"),
        P("fs", "tp"),
        P("fs", "tp"),
        P("fs", "tp"),
    )
    body = functools.partial(local, mesh.shape["fs"], mesh.shape["tp"])

    def ordered(*args):
        out = body(*args)
        return tuple(out)

    return jax.shard_map(ordered, mesh=mesh, in_specs=in_specs, out_specs=out_specs, check_vma=False)
```

time: 231 us -> 91.6 us (0.40)
  waiting for transfers between devices: 132 us -> 0 us
  Pallas kernels: 0 us -> 82.4 us
  blocking collectives: 49.8 us -> 0 us
  between operations: 15.2 us -> 0.67 us
  matrix products: 11.1 us -> 0 us
  other arithmetic: 8.26 us -> 0 us
  local copies, waits for them, and re-layouts: 13.6 us -> 8.4 us
    pallas_call x0 -> x1, Pallas kernels: none -> 82.4 us  [local(): pl.pallas_call(functools.partial(kernel, n_fs, n_tp, scale), out_shape=[s...]
    reduce_scatter x2 -> x0, waiting for transfers between devices: 66.1 us -> none  [the longest x1 43.2 us: local(): lax.psum_scatter(lax.dot_general(normed, factor_cols, (((0,), (0,)), ((),...]
    all_gather x2 -> x0, waiting for transfers between devices: 66 us -> none  [the longest x1 35.7 us: local(): projected = lax.all_gather(share, 'tp', axis=0, tiled=True)]
    psum x1 -> x0, blocking collectives: 39.5 us -> none  [local(): lax.psum((jnp.sum(key_raw * key_raw), jnp.sum(value_raw * value_raw)), ('...]
    dot_general x3 -> x0, matrix products: 11.1 us -> none  [the longest x1 6.26 us: local(): lax.dot_general(projected, cotangents.astype(jnp.float32), (((0,), (1,)),...]
    all_gather x1 -> x0, blocking collectives: 10.3 us -> none  [local(): directions = lax.all_gather(direction, 'fs', axis=0, tiled=True)]
    slice x2 -> x0, local copies, waits for them, and re-layouts: 3.4 us -> none  [the longest x1 2.7 us: local(): copies[:, key_width:]]
    convert_element_type x1 -> x0, other arithmetic: 3.3 us -> none  [local(): value_cot = (first_map.astype(jnp.float32) - row_lambda[:, None] * second...]
  transfers between devices with their start and end apart: 4 -> 0, of which waited for: 4 -> 0; matrix products, arithmetic and copies ran while one was open for 4% -> 0% of each run, Pallas kernels for 0% -> 0%
where the time goes in v1:
time: 91.6 us; the launch traced here: 91.5 us
  Pallas kernels  82.4 us (90%)
  local copies, waits for them, and re-layouts  8.4 us (9%)
    pallas_call x1, Pallas kernels, local(): pl.pallas_call(functools.partial(kernel, n_fs, n_tp, scale), out_shape=[s...  82.4 us
    unnamed x20, local copies, waits for them, and re-layouts  8.4 us

profile of v1, /device:TPU:0, one launch (start us, length us, event | category | flops | bytes accessed | tf_op | source)
XLA Modules:
  0.0 91.5 jit_solution(5987187555045731856)
XLA Ops:
  0.6 82.4 %shard_map.179 = (f32[512,256]{1,0:T(8,128)}, f32[512,256]{1,0:T(8,128)}, bf16[2048,256]{1,0:T(8,128)(2,1)}, bf16[2048,256]{1,0:T(8,128)(2,1)}, f32[64,256]{1,0:...) custom-call(bf16[256,3072]{1,0:T(8,128)(2,1)} %normed.1, bf16[256,3072]{1,0:T(8,128)(2,1)} %key_cot.1, ...), custom_call_target="tpu_custom_call" | custom-call | tf_op jit(solution)/shard_map/pallas_call | solution.py:518
  83.0 0.0 copy-start.1
  83.0 2.0 %copy.28 = f32[512,256]{1,0:T(8,128)} copy(f32[512,256]{1,0:T(8,128)} %get-tuple-element.16) | data formatting | bytes 1048576
  85.0 0.0 copy-start
  85.0 2.0 %copy.29 = f32[512,256]{1,0:T(8,128)} copy(f32[512,256]{1,0:T(8,128)} %get-tuple-element.17) | data formatting | bytes 1048576
  87.0 0.0 copy-done.1
  87.0 0.0 copy-start.5
  87.0 1.0 %copy.30 = bf16[2048,256]{1,0:T(8,128)(2,1)} copy(bf16[2048,256]{1,0:T(8,128)(2,1)S(1)} %copy-done.1) | data formatting | bytes 2097152
  87.9 0.0 copy-done
  87.9 0.0 copy-start.4
  87.9 0.0 copy-start.3
  87.9 0.0 copy-start.2
  87.9 1.0 %copy.31 = bf16[2048,256]{1,0:T(8,128)(2,1)} copy(bf16[2048,256]{1,0:T(8,128)(2,1)S(1)} %copy-done) | data formatting | bytes 2097152
  88.9 0.0 copy-done.5
  88.9 0.6 copy.32
  89.6 0.0 copy-done.4
  89.6 0.6 copy.33
  90.2 0.0 copy-done.3
  90.2 0.6 copy.34
  90.8 0.0 copy-done.2
  90.8 0.6 copy.35
Async XLA Ops:
  83.0 3.9 %copy-start.1 = (bf16[2048,256]{1,0:T(8,128)(2,1)S(1)}, bf16[2048,256]{1,0:T(8,128)(2,1)}, u32[]{:S(2)}) copy-start(bf16[2048,256]{1,0:T(8,128)(2,1)} %get-tuple-element.18) | copy-start | bytes 3145732
  85.0 2.9 %copy-start = (bf16[2048,256]{1,0:T(8,128)(2,1)S(1)}, bf16[2048,256]{1,0:T(8,128)(2,1)}, u32[]{:S(2)}) copy-start(bf16[2048,256]{1,0:T(8,128)(2,1)} %get-tuple-element.19) | copy-start | bytes 3145732
  87.0 2.0 %copy-start.5 = (f32[64,256]{1,0:T(8,128)S(1)}, f32[64,256]{1,0:T(8,128)}, u32[]{:S(2)}) copy-start(f32[64,256]{1,0:T(8,128)} %get-tuple-element.20) | copy-start | bytes 196612
  87.9 1.6 %copy-start.4 = (f32[64,256]{1,0:T(8,128)S(1)}, f32[64,256]{1,0:T(8,128)}, u32[]{:S(2)}) copy-start(f32[64,256]{1,0:T(8,128)} %get-tuple-element.21) | copy-start | bytes 196612
  87.9 2.2 %copy-start.3 = (f32[64,256]{1,0:T(8,128)S(1)}, f32[64,256]{1,0:T(8,128)}, u32[]{:S(2)}) copy-start(f32[64,256]{1,0:T(8,128)} %get-tuple-element.22) | copy-start | bytes 196612
  87.9 2.9 %copy-start.2 = (f32[64,256]{1,0:T(8,128)S(1)}, f32[64,256]{1,0:T(8,128)}, u32[]{:S(2)}) copy-start(f32[64,256]{1,0:T(8,128)} %get-tuple-element.23) | copy-start | bytes 196612

commit v2 on v1

v2 whole, which is shorter than its diff:
```python
import functools
import math

import jax
import jax.numpy as jnp
from jax import lax
from jax.experimental import pallas as pl
from jax.experimental.pallas import tpu as pltpu
from jax.sharding import PartitionSpec as P

VALUE_DIM = 256
CORES = 2
LANES = 128
TOKENS_AT_ONCE = 256
LAG = 3
MESH = pl.DeviceIdType.MESH
F32 = jnp.float32
BF16 = jnp.bfloat16


def flipped(index, bit):
    step = 1 << bit
    return index + step * (1 - 2 * ((index // step) % 2))


def split(value):
    high = value.astype(BF16)
    return high, (value - high.astype(F32)).astype(BF16)


def kernel(
    n_fs,
    n_tp,
    scale,
    normed,
    key_cot,
    first_map,
    second_map,
    lambdas,
    factor,
    key_master,
    value_master,
    key_first,
    key_second,
    value_first,
    value_second,
    masters,
    raw_out,
    moved_out,
    factors_out,
    x_v,
    kc_v,
    vc_v,
    sm_v,
    fac_v,
    ft32,
    ft_v,
    mom_v,
    own,
    away,
    sib,
    left,
    right,
    right_out,
    proj,
    key_acc,
    value_acc,
    raw,
    grain_v,
    part,
    part_in,
    moved,
    dirs,
    norms,
    in_sem,
    sib_s,
    sib_r,
    left_s,
    left_r,
    right_s,
    right_r,
    proj_s,
    proj_r,
    mast_s,
    mast_r,
    part_s,
    part_r,
    dir_s,
    dir_r,
    norm_s,
    norm_r,
    out_sem,
):
    fs = lax.axis_index("fs")
    tp = lax.axis_index("tp")
    z = tp // CORES
    core = tp % CORES
    n_z = n_tp // CORES
    features = normed.shape[0]
    width = first_map.shape[0]
    rank = factor.shape[1]
    groups, pieces, group_rows, tile = own.shape
    steps = groups * pieces
    group_fs = group_rows // n_fs
    fs_rows = key_master.shape[0]
    rank_rows = rank // n_fs
    bits = n_fs.bit_length() - 1
    other = z * CORES + (1 - core)

    loads = [
        pltpu.make_async_copy(normed, x_v, in_sem.at[0]),
        pltpu.make_async_copy(factor, fac_v, in_sem.at[1]),
        pltpu.make_async_copy(first_map, vc_v, in_sem.at[2]),
        pltpu.make_async_copy(second_map, sm_v, in_sem.at[3]),
        pltpu.make_async_copy(key_cot, kc_v, in_sem.at[4]),
        pltpu.make_async_copy(key_first, mom_v.at[0], in_sem.at[5]),
        pltpu.make_async_copy(value_first, mom_v.at[1], in_sem.at[6]),
        pltpu.make_async_copy(key_second, mom_v.at[2], in_sem.at[7]),
        pltpu.make_async_copy(value_second, mom_v.at[3], in_sem.at[8]),
    ]
    for load in loads:
        load.start()

    barrier = pltpu.get_barrier_semaphore()
    for d in range(1, n_fs):
        pl.semaphore_signal(
            barrier, inc=1, device_id=(lax.rem(fs + d, n_fs), tp), device_id_type=MESH
        )
    for d in range(1, n_tp):
        pl.semaphore_signal(
            barrier, inc=1, device_id=(fs, lax.rem(tp + d, n_tp)), device_id_type=MESH
        )
    pl.semaphore_wait(barrier, n_fs + n_tp - 2)

    def master_copy(kv, step, j):
        order = list(range(bits)) if kv == 0 else list(range(bits))[::-1]
        block = fs
        for t in range(step):
            if (j >> t) & 1:
                block = flipped(block, order[t])
        if j == 0:
            src = (key_master, value_master)[kv]
        else:
            src = masters.at[kv, block]
        slot = (1 << step) - 1 + j
        return pltpu.make_async_remote_copy(
            src_ref=src,
            dst_ref=masters.at[kv, block],
            send_sem=mast_s.at[kv, slot],
            recv_sem=mast_r.at[kv, slot],
            device_id=(flipped(fs, order[step]), tp),
            device_id_type=MESH,
        )

    for step in range(bits):
        for kv in range(2):
            master_copy(kv, step, 0).start()

    def wait_masters(step):
        for kv in range(2):
            for j in range(1 << step):
                master_copy(kv, step, j).wait_recv()

    def sib_copy(k):
        return pltpu.make_async_remote_copy(
            src_ref=away.at[:, k],
            dst_ref=sib.at[:, k],
            send_sem=sib_s.at[k],
            recv_sem=sib_r.at[k],
            device_id=(fs, other),
            device_id_type=MESH,
        )

    def left_copy(s):
        return pltpu.make_async_remote_copy(
            src_ref=left.at[s],
            dst_ref=left.at[s],
            send_sem=left_s.at[s],
            recv_sem=left_r.at[s],
            device_id=(fs, lax.rem(tp + CORES, n_tp)),
            device_id_type=MESH,
        )

    def right_copy(s):
        return pltpu.make_async_remote_copy(
            src_ref=right_out.at[s],
            dst_ref=right.at[s],
            send_sem=right_s.at[s],
            recv_sem=right_r.at[s],
            device_id=(fs, lax.rem(tp + n_tp - CORES, n_tp)),
            device_id_type=MESH,
        )

    def proj_copy(s, side):
        at = proj.at[s // pieces, side * pieces + s % pieces]
        return pltpu.make_async_remote_copy(
            src_ref=at,
            dst_ref=at,
            send_sem=proj_s.at[s],
            recv_sem=proj_r.at[s],
            device_id=(fs, other),
            device_id_type=MESH,
        )

    loads[0].wait()
    loads[1].wait()
    turned = fac_v[pl.ds(pl.multiple_of(tp * features, features), features), :].astype(F32).T
    for g in range(groups):
        for j in range(n_fs):
            row = j * rank_rows + g * group_fs
            at = g * group_rows + j * group_fs
            ft32[at : at + group_fs, :] = turned[row : row + group_fs, :]
    ft_v[...] = ft32[...].astype(BF16)

    def tokens_of(side, k):
        return pl.ds(pl.multiple_of((side * pieces + k) * tile, tile), tile)

    def project(k):
        for side, to in ((1 - core, away), (core, own)):
            out = jnp.dot(ft_v[...], x_v[:, tokens_of(side, k)], preferred_element_type=F32)
            for g in range(groups):
                to[g, k] = out[g * group_rows : (g + 1) * group_rows, :]
            if to is away:
                sib_copy(k).start()

    ahead = min(2, pieces)
    for k in range(ahead):
        project(k)

    key_acc[...] = jnp.zeros_like(key_acc)
    value_acc[...] = jnp.zeros_like(value_acc)
    span = math.gcd(width, VALUE_DIM)

    def value_cotangent(side, k):
        for b in range(width // span):
            row_lambda = lambdas[(tp * width + b * span) // VALUE_DIM]
            at = (slice(b * span, (b + 1) * span), tokens_of(side, k))
            vc_v[at] = (vc_v[at].astype(F32) - row_lambda * sm_v[at].astype(F32)).astype(BF16)

    def accumulate(g, side, k):
        cols = tokens_of(side, k)
        piece = proj[g, side * pieces + k]
        dims = (((1,), (1,)), ((), ()))
        key_acc[g] += lax.dot_general(piece, kc_v[:, cols], dims, preferred_element_type=F32)
        value_acc[g] += lax.dot_general(piece, vc_v[:, cols], dims, preferred_element_type=F32)

    def accumulate_sibling(s):
        proj_copy(s, 1 - core).wait_recv()
        accumulate(s // pieces, 1 - core, s % pieces)

    def part_copy(g, d):
        to = lax.rem(fs + d, n_fs)
        return pltpu.make_async_remote_copy(
            src_ref=part.at[g, to],
            dst_ref=part_in.at[g, d - 1],
            send_sem=part_s.at[g, d - 1],
            recv_sem=part_r.at[g, d - 1],
            device_id=(to, tp),
            device_id_type=MESH,
        )

    def send_part(g):
        for kv, acc in enumerate((key_acc, value_acc)):
            for j in range(n_fs):
                rows = pl.ds(j * group_fs, group_fs)
                lows = pl.ds(group_rows + j * group_fs, group_fs)
                part[g, j, kv] = (acc[g, rows, :] + acc[g, lows, :]) * scale
        for d in range(1, n_fs):
            part_copy(g, d).start()

    @pl.loop(0, steps + LAG * (n_z - 1))
    def _(i):
        @pl.when(i < pieces)
        def _():
            sib_copy(i).wait_recv()
            own[:, i] = own[:, i] + sib[:, i]

        s_left = i - LAG * z

        @pl.when(jnp.logical_and(s_left >= 0, s_left < steps))
        def _():
            total = own[s_left // pieces, s_left % pieces]

            @pl.when(z > 0)
            def _():
                left_copy(s_left).wait_recv()
                left[s_left] = left[s_left] + total

            @pl.when(z == 0)
            def _():
                left[s_left] = total

            @pl.when(z < n_z - 1)
            def _():
                left_copy(s_left).start()

        s_right = i - LAG * (n_z - 1 - z)

        @pl.when(jnp.logical_and(s_right >= 0, s_right < steps))
        def _():
            total = own[s_right // pieces, s_right % pieces]

            @pl.when(z < n_z - 1)
            def _():
                right_copy(s_right).wait_recv()

                @pl.when(z > 0)
                def _():
                    right_out[s_right] = right[s_right] + total

            @pl.when(z == n_z - 1)
            def _():
                right[s_right] = jnp.zeros_like(total)

                @pl.when(z > 0)
                def _():
                    right_out[s_right] = total

            @pl.when(z > 0)
            def _():
                right_copy(s_right).start()

        @pl.when(i + ahead < pieces)
        def _():
            project(i + ahead)

        @pl.when(i == 0)
        def _():
            for load in loads[2:5]:
                load.wait()

        @pl.when(i < pieces)
        def _():
            for side in range(CORES):
                value_cotangent(side, i)

        s_done = i - LAG * jnp.maximum(z, n_z - 1 - z)

        @pl.when(jnp.logical_and(s_done >= 0, s_done < steps))
        def _():
            g = s_done // pieces
            mine = core * pieces + s_done % pieces
            high, low = split(left[s_done] + right[s_done])
            proj[g, mine, 0:group_rows, :] = high
            proj[g, mine, group_rows : 2 * group_rows, :] = low
            proj_copy(s_done, core).start()

            @pl.when(s_done > 0)
            def _():
                accumulate_sibling(s_done - 1)

            @pl.when(jnp.logical_and(s_done > 0, s_done % pieces == 0))
            def _():
                send_part(g - 1)

            accumulate(g, core, s_done % pieces)

        for t in range(1, bits):

            @pl.when(i == (steps * t) // bits)
            def _():
                wait_masters(t - 1)
                for j in range(1, 1 << t):
                    for kv in range(2):
                        master_copy(kv, t, j).start()

    accumulate_sibling(steps - 1)
    send_part(groups - 1)

    def dir_copy(g, d, source):
        at = dirs.at[g, source]
        return pltpu.make_async_remote_copy(
            src_ref=at,
            dst_ref=at,
            send_sem=dir_s.at[g, d - 1],
            recv_sem=dir_r.at[g, d - 1],
            device_id=(lax.rem(fs + d, n_fs), tp),
            device_id_type=MESH,
        )

    def norm_copy(d):
        return pltpu.make_async_remote_copy(
            src_ref=norms.at[0],
            dst_ref=norms.at[d],
            send_sem=norm_s.at[d - 1],
            recv_sem=norm_r.at[d - 1],
            device_id=(fs, lax.rem(tp + d, n_tp)),
            device_id_type=MESH,
        )

    for load in loads[5:]:
        load.wait()
    for g in range(groups):
        small = part[g, fs]
        for d in range(1, n_fs):
            part_copy(g, d).wait_recv()
            small = small + part_in[g, d - 1]
        rows = slice(g * group_fs, (g + 1) * group_fs)
        first_new = 0.8 * mom_v[0:2, rows] + 0.2 * small
        second_new = 0.9 * mom_v[2:4, rows] + 0.1 * small * small
        dirs[g, fs] = first_new / (jnp.sqrt(second_new) + 1e-06)
        for d in range(1, n_fs):
            dir_copy(g, d, fs).start()
        moved[0:2, rows] = first_new
        moved[2:4, rows] = second_new
    moments = pltpu.make_async_copy(moved, moved_out, out_sem.at[0])
    moments.start()
    for g in range(groups):
        for d in range(1, n_fs):
            dir_copy(g, d, lax.rem(fs + n_fs - d, n_fs)).wait_recv()

    block = fs_rows

    def raw_copy(kv, n):
        return pltpu.make_async_copy(raw.at[kv, n], raw_out.at[kv, n], out_sem.at[2 + kv * n_fs + n])

    sums = []
    for kv in range(2):
        high, low = split(jnp.concatenate(
            [dirs[g, j, kv] for j in range(n_fs) for g in range(groups)], axis=0
        ))

        def body(n, total):
            rows = fac_v[pl.ds(pl.multiple_of(n * block, block), block), :]
            out = jnp.dot(rows, high, preferred_element_type=F32) + jnp.dot(
                rows, low, preferred_element_type=F32
            )
            raw[kv, n] = out
            raw_copy(kv, n).start()
            return total + jnp.sum((out * out).reshape(block // 8, 8, width), axis=0)

        total = lax.fori_loop(0, n_fs, body, jnp.zeros((8, width), F32))
        sums.append(jnp.sum(total))
    norms[0, 0] = jnp.full(norms.shape[2:], sums[0], F32)
    norms[0, 1] = jnp.full(norms.shape[2:], sums[1], F32)
    for d in range(1, n_tp):
        norm_copy(d).start()
    wait_masters(bits - 1)
    squares = norms[0]
    for d in range(1, n_tp):
        norm_copy(d).wait_recv()
        squares = squares + norms[d]
    cells = factor.shape[0] * width * n_tp
    grain_v[...] = 0.02 / jnp.sqrt(squares / cells + 0.01)
    factors = pltpu.make_async_copy(grain_v, factors_out, out_sem.at[1])
    factors.start()

    @pl.loop(0, pieces)
    def _(k):
        sib_copy(k).wait_send()

    @pl.loop(0, steps)
    def _(s):
        proj_copy(s, core).wait_send()

        @pl.when(z < n_z - 1)
        def _():
            left_copy(s).wait_send()

        @pl.when(z > 0)
        def _():
            right_copy(s).wait_send()

    for kv in range(2):
        for step in range(bits):
            for j in range(1 << step):
                master_copy(kv, step, j).wait_send()
    for g in range(groups):
        for d in range(1, n_fs):
            part_copy(g, d).wait_send()
            dir_copy(g, d, fs).wait_send()
    for d in range(1, n_tp):
        norm_copy(d).wait_send()
    moments.wait()
    factors.wait()
    for kv in range(2):
        for n in range(n_fs):
            raw_copy(kv, n).wait()


def finish(
    n_fs,
    masters,
    raw,
    moved,
    factors,
    key_master,
    value_master,
    key_new,
    value_new,
    key_copy,
    value_copy,
    key_first_new,
    key_second_new,
    value_first_new,
    value_second_new,
    master_v,
    raw_v,
    copy_v,
    moved_v,
    in_sem,
    out_sem,
):
    fs = lax.axis_index("fs")
    block = key_master.shape[0]

    def own_in(kv):
        src = (key_master, value_master)[kv]
        return pltpu.make_async_copy(src, master_v.at[kv, fs], in_sem.at[0, kv, fs])

    def master_in(kv, n):
        return pltpu.make_async_copy(masters.at[kv, n], master_v.at[kv, n], in_sem.at[0, kv, n])

    def raw_in(kv, n):
        return pltpu.make_async_copy(raw.at[kv, n], raw_v.at[kv, n], in_sem.at[1, kv, n])

    moved_in = pltpu.make_async_copy(moved, moved_v, out_sem.at[0])
    for kv in range(2):
        for n in range(n_fs):

            @pl.when(fs == n)
            def _():
                own_in(kv).start()

            @pl.when(fs != n)
            def _():
                master_in(kv, n).start()

            raw_in(kv, n).start()
    moved_in.start()
    outs = []
    for kv in range(2):
        grain = factors[kv, 0:1, 0:1]
        for n in range(n_fs):
            master_in(kv, n).wait()
            raw_in(kv, n).wait()
            new = 0.998 * master_v[kv, n] - grain * raw_v[kv, n]
            copy_v[kv, n] = new.astype(BF16)
            to = (key_copy, value_copy)[kv].at[pl.ds(n * block, block), :]
            outs.append(pltpu.make_async_copy(copy_v.at[kv, n], to, in_sem.at[2, kv, n]))
            outs[-1].start()

            @pl.when(fs == n)
            def _():
                raw_v[kv, n] = new

        to = (key_new, value_new)[kv]
        outs.append(pltpu.make_async_copy(raw_v.at[kv, fs], to, out_sem.at[1 + kv]))
        outs[-1].start()
    moved_in.wait()
    for n, ref in enumerate((key_first_new, value_first_new, key_second_new, value_second_new)):
        outs.append(pltpu.make_async_copy(moved_v.at[n], ref, out_sem.at[3 + n]))
        outs[-1].start()
    for out in outs:
        out.wait()


def local(n_fs, n_tp, *args):
    normed, key_cot, first_map, second_map, lambdas, factor, key_master = args[:7]
    features, tokens = normed.shape
    width = first_map.shape[0]
    rows, rank = factor.shape
    fs_rows = key_master.shape[0]
    rank_rows = rank // n_fs
    tile = TOKENS_AT_ONCE
    pieces = tokens // (CORES * tile)
    groups = max(1, min(4, rank_rows // 8))
    group_rows = rank // groups
    group_fs = rank_rows // groups
    steps = groups * pieces
    gathered = (2, n_fs, fs_rows, width)
    scale = 1.0 / math.sqrt(tokens * n_fs)
    any_spec = pl.BlockSpec(memory_space=pl.ANY)
    specs = [any_spec] * 12
    specs[4] = pl.BlockSpec(memory_space=pltpu.SMEM)
    dma = pltpu.SemaphoreType.DMA
    sds = jax.ShapeDtypeStruct
    small = sds((rank_rows, width), F32)
    masters, raw, moved, factors = pl.pallas_call(
        functools.partial(kernel, n_fs, n_tp, scale),
        out_shape=[
            sds(gathered, F32),
            sds(gathered, F32),
            sds((4, rank_rows, width), F32),
            sds((2, 8, LANES), F32),
        ],
        in_specs=specs,
        out_specs=[any_spec] * 4,
        scratch_shapes=[
            pltpu.VMEM((features, tokens), BF16),
            pltpu.VMEM((width, tokens), BF16),
            pltpu.VMEM((width, tokens), BF16),
            pltpu.VMEM((width, tokens), BF16),
            pltpu.VMEM((rows, rank), BF16),
            pltpu.VMEM((rank, features), F32),
            pltpu.VMEM((rank, features), BF16),
            pltpu.VMEM((4, rank_rows, width), F32),
            pltpu.VMEM((groups, pieces, group_rows, tile), F32),
            pltpu.VMEM((groups, pieces, group_rows, tile), F32),
            pltpu.VMEM((groups, pieces, group_rows, tile), F32),
            pltpu.VMEM((steps, group_rows, tile), F32),
            pltpu.VMEM((steps, group_rows, tile), F32),
            pltpu.VMEM((steps, group_rows, tile), F32),
            pltpu.VMEM((groups, CORES * pieces, 2 * group_rows, tile), BF16),
            pltpu.VMEM((groups, 2 * group_rows, width), F32),
            pltpu.VMEM((groups, 2 * group_rows, width), F32),
            pltpu.VMEM(gathered, F32),
            pltpu.VMEM((2, 8, LANES), F32),
            pltpu.VMEM((groups, n_fs, 2, group_fs, width), F32),
            pltpu.VMEM((groups, n_fs - 1, 2, group_fs, width), F32),
            pltpu.VMEM((4, rank_rows, width), F32),
            pltpu.VMEM((groups, n_fs, 2, group_fs, width), F32),
            pltpu.VMEM((n_tp, 2, 8, LANES), F32),
            dma((9,)),
            dma((pieces,)),
            dma((pieces,)),
            dma((steps,)),
            dma((steps,)),
            dma((steps,)),
            dma((steps,)),
            dma((steps,)),
            dma((steps,)),
            dma((2, n_fs - 1)),
            dma((2, n_fs - 1)),
            dma((groups, n_fs - 1)),
            dma((groups, n_fs - 1)),
            dma((groups, n_fs - 1)),
            dma((groups, n_fs - 1)),
            dma((n_tp - 1,)),
            dma((n_tp - 1,)),
            dma((2 + 2 * n_fs,)),
        ],
        compiler_params=pltpu.CompilerParams(
            collective_id=0, has_side_effects=True, vmem_limit_bytes=40 * 1024 * 1024
        ),
    )(*args)
    vmem_spec = pl.BlockSpec(memory_space=pltpu.VMEM)
    return pl.pallas_call(
        functools.partial(finish, n_fs),
        out_shape=[
            sds((fs_rows, width), F32),
            sds((fs_rows, width), F32),
            sds((rows, width), BF16),
            sds((rows, width), BF16),
            small,
            small,
            small,
            small,
        ],
        in_specs=[any_spec, any_spec, any_spec, vmem_spec, any_spec, any_spec],
        out_specs=[any_spec] * 8,
        scratch_shapes=[
            pltpu.VMEM(gathered, F32),
            pltpu.VMEM(gathered, F32),
            pltpu.VMEM(gathered, BF16),
            pltpu.VMEM((4, rank_rows, width), F32),
            dma((3, 2, n_fs)),
            dma((7,)),
        ],
        compiler_params=pltpu.CompilerParams(vmem_limit_bytes=20 * 1024 * 1024),
    )(masters, raw, moved, factors, key_master, args[7])


def solution(mesh):
    in_specs = (
        P("tp", "fs"),
        P("tp", "fs"),
        P("tp", "fs"),
        P("tp", "fs"),
        P(),
        P(),
        P("fs", "tp"),
        P("fs", "tp"),
        P("fs", "tp"),
        P("fs", "tp"),
        P("fs", "tp"),
        P("fs", "tp"),
    )
    out_specs = (
        P("fs", "tp"),
        P("fs", "tp"),
        P(None, "tp"),
        P(None, "tp"),
        P("fs", "tp"),
        P("fs", "tp"),
        P("fs", "tp"),
        P("fs", "tp"),
    )
    body = functools.partial(local, mesh.shape["fs"], mesh.shape["tp"])

    def ordered(*args):
        out = body(*args)
        return tuple(out)

    return jax.shard_map(ordered, mesh=mesh, in_specs=in_specs, out_specs=out_specs, check_vma=False)
```

time: 91.6 us -> 90.1 us (0.984)
  Pallas kernels: 82.4 us -> 73.8 us
  local copies, waits for them, and re-layouts: 8.4 us -> 15.1 us
    pallas_call x1, Pallas kernels: 82.4 us -> 71 us  [local(): pl.pallas_call(functools.partial(kernel, n_fs, n_tp, scale), out_shape=[s...]
    unnamed x20 -> x26, local copies, waits for them, and re-layouts: 8.4 us -> 15.1 us
    pallas_call x0 -> x1, Pallas kernels: none -> 2.8 us  [local(): pl.pallas_call(functools.partial(finish, n_fs), out_shape=[sds((fs_rows,...]
where the time goes in v2:
time: 90.1 us; the launch traced here: 89.5 us
  Pallas kernels  73.8 us (82%)
  local copies, waits for them, and re-layouts  15.1 us (17%)
    pallas_call x1, Pallas kernels, local(): pl.pallas_call(functools.partial(kernel, n_fs, n_tp, scale), out_shape=[s...  71 us
    unnamed x26, local copies, waits for them, and re-layouts  15.1 us
    pallas_call x1, Pallas kernels, local(): pl.pallas_call(functools.partial(finish, n_fs), out_shape=[sds((fs_rows,...  2.8 us

profile of v2, /device:TPU:0, one launch (start us, length us, event | category | flops | bytes accessed | tf_op | source)
XLA Modules:
  0.0 89.5 jit_solution(14165093216063099808)
XLA Ops:
  0.6 0.0 copy-start.1
  0.6 1.0 %copy-done.1 = f32[512,256]{1,0:T(8,128)S(1)} copy-done((f32[512,256]{1,0:T(8,128)S(1)}, f32[512,256]{1,0:T(8,128)}, u32[]{:S(2)}) %copy-start.1) | copy-done | bytes 524312
  1.7 0.0 copy-start.2
  1.7 1.0 %copy-done.2 = f32[512,256]{1,0:T(8,128)S(1)} copy-done((f32[512,256]{1,0:T(8,128)S(1)}, f32[512,256]{1,0:T(8,128)}, u32[]{:S(2)}) %copy-start.2) | copy-done | bytes 524312
  2.7 0.0 copy-start.3
  2.7 1.4 %copy-done.3 = bf16[256,3072]{1,0:T(8,128)(2,1)S(1)} copy-done((bf16[256,3072]{1,0:T(8,128)(2,1)S(1)}, bf16[256,3072]{1,0:T(8,128)(2,1)}, u32[]{:S(2)}) %copy-start.3) | copy-done | bytes 1572888
  4.1 0.0 copy-start.4
  4.1 1.4 %copy-done.4 = bf16[256,3072]{1,0:T(8,128)(2,1)S(1)} copy-done((bf16[256,3072]{1,0:T(8,128)(2,1)S(1)}, bf16[256,3072]{1,0:T(8,128)(2,1)}, u32[]{:S(2)}) %copy-start.4) | copy-done | bytes 1572888
  5.5 0.0 copy-start.5
  5.5 1.4 %copy-done.5 = bf16[256,3072]{1,0:T(8,128)(2,1)S(1)} copy-done((bf16[256,3072]{1,0:T(8,128)(2,1)S(1)}, bf16[256,3072]{1,0:T(8,128)(2,1)}, u32[]{:S(2)}) %copy-start.5) | copy-done | bytes 1572888
  6.9 0.0 copy-start.6
  7.0 1.4 %copy-done.6 = bf16[256,3072]{1,0:T(8,128)(2,1)S(1)} copy-done((bf16[256,3072]{1,0:T(8,128)(2,1)S(1)}, bf16[256,3072]{1,0:T(8,128)(2,1)}, u32[]{:S(2)}) %copy-start.6) | copy-done | bytes 1572888
  8.4 0.0 copy-start.7
  8.4 1.2 %copy-done.7 = bf16[2048,256]{1,0:T(8,128)(2,1)S(1)} copy-done((bf16[2048,256]{1,0:T(8,128)(2,1)S(1)}, bf16[2048,256]{1,0:T(8,128)(2,1)}, u32[]{:S(2)}) %copy-start.7) | copy-done | bytes 1048600
  9.6 0.0 copy-start.8
  9.6 0.8 copy-done.8
  10.4 0.0 copy-start.9
  10.4 0.8 copy-done.9
  11.3 0.0 copy-start.10
  11.3 0.8 copy-done.10
  12.1 0.0 copy-start.11
  12.1 0.8 copy-done.11
  12.9 0.0 copy-start.12
  12.9 0.7 copy-done.12
  13.6 71.0 %shard_map.179 = (f32[2,4,512,256]{3,2,1,0:T(8,128)S(1)}, f32[2,4,512,256]{3,2,1,0:T(8,128)}, f32[4,64,256]{2,1,0:T(8,128)S(1)}, f32[2,8,128]{2,1,0:T(8,128)S(1)}) custom-call(bf16[256,3072]{1,0:T(8,128)(2,1)S(1)} %copy-done.3, bf16[256,3072]{1,0:T(8,128)(2,1)S(1)} %copy-done.4, bf16[256,3072]{1,0:T(8,128)(2,1)S(1)} %copy-done.5, ...), custom_call_target="tpu_custom_call" | custom-call | tf_op jit(solution)/shard_map/pallas_call | solution.py:579
  84.6 0.0 copy-start
  84.6 2.2 %copy-done = f32[2,4,512,256]{3,2,1,0:T(8,128)S(1)} copy-done((f32[2,4,512,256]{3,2,1,0:T(8,128)S(1)}, f32[2,4,512,256]{3,2,1,0:T(8,128)}, u32[]{:S(2)}) %copy-start) | copy-done | bytes 4194328
  86.7 2.8 %shard_map.180 = (f32[512,256]{1,0:T(8,128)}, f32[512,256]{1,0:T(8,128)}, bf16[2048,256]{1,0:T(8,128)(2,1)}, bf16[2048,256]{1,0:T(8,128)(2,1)}, f32[64,256]{1,0:...) custom-call(f32[2,4,512,256]{3,2,1,0:T(8,128)S(1)} %get-tuple-element.12.masters, ...), custom_call_target="tpu_custom_call" | custom-call | tf_op jit(solution)/shard_map/pallas_call | solution.py:638
Async XLA Ops:
  0.6 1.0 %copy-start.1 = (f32[512,256]{1,0:T(8,128)S(1)}, f32[512,256]{1,0:T(8,128)}, u32[]{:S(2)}) copy-start(f32[512,256]{1,0:T(8,128)} %key_master.3) | copy-start | bytes 1572868
  1.7 1.0 %copy-start.2 = (f32[512,256]{1,0:T(8,128)S(1)}, f32[512,256]{1,0:T(8,128)}, u32[]{:S(2)}) copy-start(f32[512,256]{1,0:T(8,128)} %value_master.3) | copy-start | bytes 1572868
  2.7 1.4 %copy-start.3 = (bf16[256,3072]{1,0:T(8,128)(2,1)S(1)}, bf16[256,3072]{1,0:T(8,128)(2,1)}, u32[]{:S(2)}) copy-start(bf16[256,3072]{1,0:T(8,128)(2,1)} %normed.1) | copy-start | bytes 4718596
  4.1 1.4 %copy-start.4 = (bf16[256,3072]{1,0:T(8,128)(2,1)S(1)}, bf16[256,3072]{1,0:T(8,128)(2,1)}, u32[]{:S(2)}) copy-start(bf16[256,3072]{1,0:T(8,128)(2,1)} %key_cot.1) | copy-start | bytes 4718596
  5.5 1.4 %copy-start.5 = (bf16[256,3072]{1,0:T(8,128)(2,1)S(1)}, bf16[256,3072]{1,0:T(8,128)(2,1)}, u32[]{:S(2)}) copy-start(bf16[256,3072]{1,0:T(8,128)(2,1)} %first_map.1) | copy-start | bytes 4718596
  6.9 1.4 %copy-start.6 = (bf16[256,3072]{1,0:T(8,128)(2,1)S(1)}, bf16[256,3072]{1,0:T(8,128)(2,1)}, u32[]{:S(2)}) copy-start(bf16[256,3072]{1,0:T(8,128)(2,1)} %second_map.1) | copy-start | bytes 4718596
  8.4 1.2 %copy-start.7 = (bf16[2048,256]{1,0:T(8,128)(2,1)S(1)}, bf16[2048,256]{1,0:T(8,128)(2,1)}, u32[]{:S(2)}) copy-start(bf16[2048,256]{1,0:T(8,128)(2,1)} %factor.1) | copy-start | bytes 3145732
  9.6 0.8 copy-start.8
  10.4 0.8 copy-start.9
  11.3 0.8 copy-start.10
  12.1 0.8 copy-start.11
  12.9 0.7 copy-start.12
  84.6 2.2 %copy-start = (f32[2,4,512,256]{3,2,1,0:T(8,128)S(1)}, f32[2,4,512,256]{3,2,1,0:T(8,128)}, u32[]{:S(2)}) copy-start(f32[2,4,512,256]{3,2,1,0:T(8,128)} %get-tuple-element.13.raw) | copy-start | bytes 12582916

commit v3 on v2

--- a/solution.py
+++ b/solution.py
@@ -631,7 +631,7 @@
             dma((2 + 2 * n_fs,)),
         ],
         compiler_params=pltpu.CompilerParams(
-            collective_id=0, has_side_effects=True, vmem_limit_bytes=40 * 1024 * 1024
+            collective_id=0, has_side_effects=True, vmem_limit_bytes=63 * 1024 * 1024
         ),
     )(*args)
     vmem_spec = pl.BlockSpec(memory_space=pltpu.VMEM)
@@ -657,7 +657,7 @@
             dma((3, 2, n_fs)),
             dma((7,)),
         ],
-        compiler_params=pltpu.CompilerParams(vmem_limit_bytes=20 * 1024 * 1024),
+        compiler_params=pltpu.CompilerParams(vmem_limit_bytes=63 * 1024 * 1024),
     )(masters, raw, moved, factors, key_master, args[7])
 
 

time: 90.1 us -> 77.4 us (0.86)
  local copies, waits for them, and re-layouts: 15.1 us -> 0 us
  Pallas kernels: 73.8 us -> 76.5 us
    unnamed x26 -> x0, local copies, waits for them, and re-layouts: 15.1 us -> none
    pallas_call x1, Pallas kernels: 2.8 us -> 6.02 us  [local(): pl.pallas_call(functools.partial(finish, n_fs), out_shape=[sds((fs_rows,...]
where the time goes in v3:
time: 77.4 us; the launch traced here: 77.2 us
  Pallas kernels  76.5 us (99%)
    pallas_call x1, Pallas kernels, local(): pl.pallas_call(functools.partial(kernel, n_fs, n_tp, scale), out_shape=[s...  70.5 us
    pallas_call x1, Pallas kernels, local(): pl.pallas_call(functools.partial(finish, n_fs), out_shape=[sds((fs_rows,...  6.02 us

profile of v3, /device:TPU:0, one launch (start us, length us, event | category | flops | bytes accessed | tf_op | source)
XLA Modules:
  0.0 77.2 jit_solution(6773748945028780452)
XLA Ops:
  0.6 70.5 %shard_map.179 = (f32[2,4,512,256]{3,2,1,0:T(8,128)}, f32[2,4,512,256]{3,2,1,0:T(8,128)}, f32[4,64,256]{2,1,0:T(8,128)}, f32[2,8,128]{2,1,0:T(8,128)}) custom-call(bf16[256,3072]{1,0:T(8,128)(2,1)} %normed.1, bf16[256,3072]{1,0:T(8,128)(2,1)} %key_cot.1, bf16[256,3072]{1,0:T(8,128)(2,1)} %first_map.1, bf16[256,3072]{1,0:T(8,128)(2,1)} %second_map.1, ...), custom_call_target="tpu_custom_call" | custom-call | tf_op jit(solution)/shard_map/pallas_call | solution.py:579
  71.2 6.0 %shard_map.180 = (f32[512,256]{1,0:T(8,128)}, f32[512,256]{1,0:T(8,128)}, bf16[2048,256]{1,0:T(8,128)(2,1)}, bf16[2048,256]{1,0:T(8,128)(2,1)}, f32[64,256]{1,0:...) custom-call(f32[2,4,512,256]{3,2,1,0:T(8,128)} %get-tuple-element.12.masters, ...), custom_call_target="tpu_custom_call" | custom-call | tf_op jit(solution)/shard_map/pallas_call | solution.py:638
